TPU v7x, 512 devices: a whole 4x4x16 slice. The times are simulated.
512 devices in a mesh: fs: 16 (over y, x), tp: 32 (over z, core).
Axes of the slice: x: 4, y: 4, z: 16, core: 2. Of those that a mesh axis runs over, the one named last changes fastest.
Arguments:
- saved_input: bfloat16 [16384, 4096], P('fs', 'tp'), may hold values from -6 to 6
- query_cot: bfloat16 [16384, 4096], P('fs', 'tp'), may hold values from -6 to 6
- key_cot: bfloat16 [16384, 4096], P('fs', 'tp'), may hold values from -6 to 6
- query_master: float32 [4096, 4096], P('fs', 'tp'), may hold values from -0.09375 to 0.09375
- key_master: float32 [4096, 4096], P('fs', 'tp'), may hold values from -0.09375 to 0.09375
- query_basis: bfloat16 [4096, 256], P('fs'), may hold values from -3 to 3
- key_basis: bfloat16 [4096, 256], P('fs'), may hold values from -3 to 3
- query_first: float32 [256, 4096], P('fs', 'tp'), may hold values from -240 to 240
- query_second: float32 [256, 4096], P('fs', 'tp'), may hold values from 1000 to 20000
- key_first: float32 [256, 4096], P('fs', 'tp'), may hold values from -240 to 240
- key_second: float32 [256, 4096], P('fs', 'tp'), may hold values from 1000 to 20000
Outputs:
- query_step: float32 [4096, 4096], P('fs', 'tp')
- query_weight: float32 [4096, 4096], P('fs', 'tp')
- query_copy: bfloat16 [4096, 4096], P(None, 'tp')
- query_first_new: float32 [256, 4096], P('fs', 'tp')
- query_second_new: float32 [256, 4096], P('fs', 'tp')
- key_step: float32 [4096, 4096], P('fs', 'tp')
- key_weight: float32 [4096, 4096], P('fs', 'tp')
- key_copy: bfloat16 [4096, 4096], P(None, 'tp')
- key_first_new: float32 [256, 4096], P('fs', 'tp')
- key_second_new: float32 [256, 4096], P('fs', 'tp')
All inputs are finite; a program needn't handle non-finite values.
Results may differ from a plain program's by a relative error of at most 0.0065.
Values may be sent and summed in bfloat16 or wider, within the bound.
A program may use at most 64 MiB of HBM per device.

v0:
```python
import functools

import jax
import jax.numpy as jnp
from jax import lax
from jax.experimental import pallas as pl
from jax.experimental.pallas import tpu as pltpu
from jax.sharding import PartitionSpec as P

HD = 128

moment_decay = 0.8
square_decay = 0.9
square_floor = 1.0
norm_floor = 0.01
step_rate = 0.01

BF = jnp.bfloat16
F32 = jnp.float32
MESH = pl.DeviceIdType.MESH


def exchange_kernel(
    fs,
    tp,
    x_hbm,
    qc_hbm,
    kc_hbm,
    qm_hbm,
    km_hbm,
    qb_hbm,
    kb_hbm,
    qf_ref,
    qs_ref,
    kf_ref,
    ks_ref,
    qfn_ref,
    qsn_ref,
    kfn_ref,
    ksn_ref,
    ratio_ref,
    scale_ref,
    gathered,
    basis_out,
    basis,
    x_v,
    cot,
    master,
    rounded,
    half_send,
    half_recv,
    half_own,
    z_send,
    z_recv,
    low,
    proj,
    proj_send,
    proj_recv,
    load_sem,
    b_send,
    b_recv,
    d_send,
    d_recv,
    p_send,
    p_recv,
    zr_send,
    zr_recv,
    zg_send,
    zg_recv,
    pf_send,
    pf_recv,
    rs_send,
    rs_recv,
    ag_send,
    ag_recv,
    m_send,
    m_recv,
    out_sem,
):
    f = lax.axis_index("fs")
    t = lax.axis_index("tp")
    z, c = t // 2, t % 2
    depth = tp // 2
    relay = fs == 4
    rows, rank = qb_hbm.shape
    width = qc_hbm.shape[1]
    tokens, columns = x_v.shape
    part = rank // fs
    half_rows = rows // 2
    half = tokens // 2
    chunk = tokens // tp

    def at(start, size):
        return pl.ds(pl.multiple_of(start, size), size)

    def remote(src, dst, send, recv, df, dt):
        return pltpu.make_async_remote_copy(
            src_ref=src,
            dst_ref=dst,
            send_sem=send,
            recv_sem=recv,
            device_id=(df, dt),
            device_id_type=MESH,
        )

    loads = [
        pltpu.make_async_copy(qb_hbm, basis.at[0, at(f * rows, rows)], load_sem.at[0]),
        pltpu.make_async_copy(kb_hbm, basis.at[1, at(f * rows, rows)], load_sem.at[1]),
        pltpu.make_async_copy(qm_hbm, master.at[0], load_sem.at[2]),
        pltpu.make_async_copy(km_hbm, master.at[1], load_sem.at[3]),
        pltpu.make_async_copy(x_hbm, x_v, load_sem.at[4]),
        pltpu.make_async_copy(qc_hbm, cot.at[0], load_sem.at[5]),
        pltpu.make_async_copy(kc_hbm, cot.at[1], load_sem.at[6]),
    ]
    for load in loads:
        load.start()

    barrier = pltpu.get_barrier_semaphore()
    for m in range(1, fs):
        pl.semaphore_signal(barrier, inc=1, device_id=(f ^ m, t), device_id_type=MESH)
    pl.semaphore_signal(barrier, inc=1, device_id=(f, t ^ 1), device_id_type=MESH)
    for d in range(1, depth):
        other = lax.rem(z + d, depth) * 2 + c
        pl.semaphore_signal(barrier, inc=1, device_id=(f, other), device_id_type=MESH)
    loads[0].wait()
    loads[1].wait()
    pl.semaphore_wait(barrier, fs - 1 + depth)

    def basis_copy(j, m, owner, target):
        piece = basis.at[j, at(owner * rows + c * half_rows, half_rows)]
        return remote(piece, piece, b_send.at[m, j], b_recv.at[m, j], target, t)

    direct = [m for m in range(1, fs) if not (relay and m == 3)]
    basis_copies = {}
    for m in direct:
        for j in (0, 1) if m % 2 else (1, 0):
            basis_copies[m, j] = basis_copy(j, m, f, f ^ m)
            basis_copies[m, j].start()

    loads[2].wait()
    loads[3].wait()
    tile = min(rows, 128)

    for j in range(2):

        @pl.loop(0, rows // tile)
        def _(i, j=j):
            place = at(i * tile, tile)
            rounded[j, place, :] = master[j, place, :].astype(BF)

    def master_copy(j, m):
        return remote(
            rounded.at[j],
            gathered.at[j, at(f * rows, rows)],
            m_send.at[m, j],
            m_recv.at[m, j],
            f ^ m,
            t,
        )

    def master_relay(j, side):
        source = 1 + j
        piece = gathered.at[j, at((f ^ source) * rows + side * half_rows, half_rows)]
        slot = 3 + side
        return remote(piece, piece, m_send.at[slot, j], m_recv.at[slot, j], f ^ (2 - j), t)

    if relay:
        basis_copies[1, 0].wait_recv()
        basis_copies[3, 0] = basis_copy(0, 3, f ^ 1, f ^ 2)
        basis_copies[3, 0].start()
        basis_copies[2, 1].wait_recv()
        basis_copies[3, 1] = basis_copy(1, 3, f ^ 2, f ^ 1)
        basis_copies[3, 1].start()

    master_copies = {}
    for turn in range(2):
        for m in direct:
            j = (m + 1 + turn) % 2
            master_copies[m, j] = master_copy(j, m)
            master_copies[m, j].start()
    kept = pltpu.make_async_copy(rounded, gathered.at[:, at(f * rows, rows)], out_sem.at[1])
    kept.start()

    waited = {(1, 0), (2, 1)} if relay else set()
    for m in range(1, fs):
        for j in range(2):
            if (m, j) not in waited:
                basis_copies[m, j].wait_recv()

    loads[4].wait()
    step = min(half, 256)

    def project(start, j):
        return jnp.dot(
            x_v[at(start, step), :],
            basis[j, at(t * columns, columns), :],
            preferred_element_type=F32,
        )

    for j in range(2):

        @pl.loop(0, half // step)
        def _(i, j=j):
            half_send[at(i * step, step), j * rank : (j + 1) * rank] = project(
                (1 - c) * half + i * step, j
            ).astype(BF)

    swap = remote(half_send, half_recv, p_send, p_recv, f, t ^ 1)
    swap.start()
    for j in range(2):

        @pl.loop(0, half // step)
        def _(i, j=j):
            half_own[at(i * step, step), j * rank : (j + 1) * rank] = project(
                c * half + i * step, j
            )

    swap.wait_recv()

    partner_copies = []
    for m in range(1, fs):
        piece = basis.at[:, at((f ^ m) * rows + c * half_rows, half_rows)]
        copy = remote(piece, piece, d_send.at[m], d_recv.at[m], f, t ^ 1)
        copy.start()
        partner_copies.append(copy)

    @pl.loop(0, half // chunk)
    def _(i):
        place = at(i * chunk, chunk)
        both = half_own[place, :] + half_recv[place, :].astype(F32)
        half_own[place, :] = both
        z_send[place, :] = both.astype(BF)

    z_copies = []
    for d in range(1, depth):
        other = lax.rem(z + d, depth)
        copy = remote(
            z_send.at[at(other * chunk, chunk)],
            z_recv.at[d],
            zr_send.at[d],
            zr_recv.at[d],
            f,
            other * 2 + c,
        )
        copy.start()
        z_copies.append(copy)
    total = half_own[at(z * chunk, chunk), :]
    for d in range(1, depth):
        z_copies[d - 1].wait_recv()
        total = total + z_recv[d].astype(F32)
    low[at(c * half + z * chunk, chunk), :] = total.astype(BF)

    def low_piece(d, core):
        return low.at[at(core * half + lax.rem(z + depth - d, depth) * chunk, chunk)]

    g_copies = []
    for d in range(1, depth):
        other = lax.rem(z + d, depth)
        copy = remote(
            low_piece(0, c), low_piece(0, c), zg_send.at[d], zg_recv.at[d], f, other * 2 + c
        )
        copy.start()
        g_copies.append(copy)
    forwards = []
    for d in range(depth):
        if d > 0:
            g_copies[d - 1].wait_recv()
        copy = remote(low_piece(d, c), low_piece(d, c), pf_send.at[d], pf_recv.at[d], f, t ^ 1)
        copy.start()
        forwards.append(copy)
    loads[5].wait()
    loads[6].wait()
    for copy in forwards:
        copy.wait_recv()

    for j in range(2):
        product = lax.dot_general(
            low[:, j * rank : (j + 1) * rank],
            cot[j],
            (((0,), (0,)), ((), ())),
            preferred_element_type=F32,
        )
        proj[j] = product
        proj_send[j] = product.astype(BF)
    r_copies = []
    for m in range(1, fs):
        copy = remote(
            proj_send.at[:, at((f ^ m) * part, part)],
            proj_recv.at[m],
            rs_send.at[m],
            rs_recv.at[m],
            f ^ m,
            t,
        )
        copy.start()
        r_copies.append(copy)
    if relay:
        for j in range(2):
            master_copies[1 + j, j].wait_recv()
            master_copies[3, j] = master_relay(j, 0)
            master_copies[3, j].start()
    for copy in r_copies:
        copy.wait_recv()

    own = at(f * part, part)
    moments = ((qf_ref, qs_ref, qfn_ref, qsn_ref), (kf_ref, ks_ref, kfn_ref, ksn_ref))
    for j, (first, second, first_out, second_out) in enumerate(moments):
        summed = proj[j, own, :]
        for m in range(1, fs):
            summed = summed + proj_recv[m, j].astype(F32)
        first_new = moment_decay * first[...] + (1.0 - moment_decay) * summed
        second_new = square_decay * second[...] + (1.0 - square_decay) * summed * summed
        first_out[...] = first_new
        second_out[...] = second_new
        ratio_ref[j, own, :] = (first_new / jnp.sqrt(second_new + square_floor)).astype(BF)

    a_copies = []
    for m in range(1, fs):
        piece = ratio_ref.at[:, own]
        copy = remote(piece, piece, ag_send.at[m], ag_recv.at[m], f ^ m, t)
        copy.start()
        a_copies.append(copy)

    if relay:
        for j in range(2):
            master_copies[4, j] = master_relay(j, 1)
            master_copies[4, j].start()

    for copy in partner_copies:
        copy.wait_recv()
    store = pltpu.make_async_copy(basis, basis_out, out_sem.at[0])
    store.start()
    for copy in a_copies:
        copy.wait_recv()

    high = min(rows, 256)
    for j in range(2):

        def add(i, total, j=j):
            update = jnp.dot(
                basis[j, at(i * high, high), :], ratio_ref[j], preferred_element_type=F32
            )
            return total + jnp.sum((update * update).reshape(high // 8, 8, width), axis=0)

        sums = lax.fori_loop(0, fs * rows // high, add, jnp.zeros((8, width), F32))
        sums = jnp.sum(sums, axis=0, keepdims=True)
        for h in range(width // HD):
            head = slice(h * HD, (h + 1) * HD)
            total = jnp.sum(sums[:, head], axis=1, keepdims=True)
            scale = 1.0 / jnp.sqrt(total / (fs * rows * HD) + norm_floor)
            scale_ref[j, :, head] = jnp.broadcast_to(scale, (8, HD))

    store.wait()
    kept.wait()
    early = {(1, 0), (2, 1)} if relay else set()
    for place, copy in master_copies.items():
        if place not in early:
            copy.wait_recv()
    for copy in list(basis_copies.values()) + partner_copies + [swap] + z_copies:
        copy.wait_send()
    for copy in g_copies + forwards + r_copies + a_copies + list(master_copies.values()):
        copy.wait_send()


def final_kernel(*refs):
    scale_ref, ratio_ref, basis_ref, gathered_ref = refs[:4]
    inputs, moments, outs, moments_out = refs[4:8], refs[8:12], refs[12:18], refs[18:]
    for j in range(2):
        scale = scale_ref[j, 0:1, :]
        own_basis, master = inputs[2 * j : 2 * j + 2]
        step_out, weight_out, copy_out = outs[3 * j : 3 * j + 3]
        update = jnp.dot(own_basis[...], ratio_ref[j], preferred_element_type=F32)
        step = update * scale
        step_out[...] = step
        weight_out[...] = master[...] - step_rate * step
        update = jnp.dot(basis_ref[j], ratio_ref[j], preferred_element_type=F32)
        step = update * scale
        copy_out[...] = (gathered_ref[j].astype(F32) - step_rate * step).astype(BF)

    @pl.when(pl.program_id(0) == 0)
    def _():
        for source, target in zip(moments, moments_out):
            target[...] = source[...]


def body(fs, tp, *args):
    saved_input, query_cot, _, query_master, key_master, query_basis, key_basis = args[:7]
    rows, rank = query_basis.shape
    tokens, columns = saved_input.shape
    width = query_cot.shape[1]
    part = rank // fs
    depth = tp // 2
    count = fs * rows
    half, chunk = tokens // 2, tokens // tp
    any_spec = pl.BlockSpec(memory_space=pl.ANY)
    vmem = pl.BlockSpec(memory_space=pltpu.VMEM)
    dma = pltpu.SemaphoreType.DMA
    moment = jax.ShapeDtypeStruct((part, width), F32)
    pairs = []
    for shape in ((fs, 2), (fs,), (), (depth,), (depth,), (depth,), (fs,), (fs,), (fs + 1, 2)):
        pairs += [dma(shape), dma(shape)]
    results = pl.pallas_call(
        functools.partial(exchange_kernel, fs, tp),
        name="exchange",
        out_shape=(
            moment,
            moment,
            moment,
            moment,
            jax.ShapeDtypeStruct((2, rank, width), BF),
            jax.ShapeDtypeStruct((2, 8, width), F32),
            jax.ShapeDtypeStruct((2, count, width), BF),
            jax.ShapeDtypeStruct((2, count, rank), BF),
        ),
        in_specs=[any_spec] * 7 + [vmem] * 4,
        out_specs=(vmem,) * 6 + (any_spec,) * 2,
        scratch_shapes=[
            pltpu.VMEM((2, count, rank), BF),
            pltpu.VMEM((tokens, columns), BF),
            pltpu.VMEM((2, tokens, width), BF),
            pltpu.VMEM((2, rows, width), F32),
            pltpu.VMEM((2, rows, width), BF),
            pltpu.VMEM((half, 2 * rank), BF),
            pltpu.VMEM((half, 2 * rank), BF),
            pltpu.VMEM((half, 2 * rank), F32),
            pltpu.VMEM((half, 2 * rank), BF),
            pltpu.VMEM((depth, chunk, 2 * rank), BF),
            pltpu.VMEM((tokens, 2 * rank), BF),
            pltpu.VMEM((2, rank, width), F32),
            pltpu.VMEM((2, rank, width), BF),
            pltpu.VMEM((fs, 2, part, width), BF),
            dma((7,)),
            *pairs,
            dma((2,)),
        ],
        compiler_params=pltpu.CompilerParams(
            collective_id=0, has_side_effects=True, vmem_limit_bytes=60 * 1024 * 1024
        ),
    )(*args)
    moments, (ratio, scale, gathered, basis) = results[:4], results[4:]

    steps = min(8, rows // 16)
    own_tile, tile = rows // steps, count // steps

    def row(i):
        return (i, 0)

    def pair(i):
        return (0, i, 0)

    def whole(i):
        return (0, 0, 0)

    own_spec = pl.BlockSpec((own_tile, width), row)
    full_spec = pl.BlockSpec((tile, width), row)
    basis_spec = pl.BlockSpec((own_tile, rank), row)
    moment_spec = pl.BlockSpec((part, width), lambda i: (0, 0))
    big = jax.ShapeDtypeStruct((rows, width), F32)
    copied = jax.ShapeDtypeStruct((count, width), BF)
    outs = pl.pallas_call(
        final_kernel,
        name="final",
        out_shape=(big, big, copied) * 2 + (moment,) * 4,
        grid=(steps,),
        in_specs=[
            pl.BlockSpec((2, 8, width), whole),
            pl.BlockSpec((2, rank, width), whole),
            pl.BlockSpec((2, tile, rank), pair),
            pl.BlockSpec((2, tile, width), pair),
            basis_spec,
            own_spec,
            basis_spec,
            own_spec,
        ]
        + [moment_spec] * 4,
        out_specs=(own_spec, own_spec, full_spec) * 2 + (moment_spec,) * 4,
        compiler_params=pltpu.CompilerParams(vmem_limit_bytes=60 * 1024 * 1024),
    )(scale, ratio, basis, gathered, query_basis, query_master, key_basis, key_master, *moments)
    return (*outs[:3], *outs[6:8], *outs[3:6], *outs[8:])


def solution(mesh):
    split, tall, wide = P("fs", "tp"), P("fs", None), P(None, "tp")
    outs = (split, split, wide, split, split)
    return jax.shard_map(
        functools.partial(body, mesh.shape["fs"], mesh.shape["tp"]),
        mesh=mesh,
        in_specs=(split,) * 5 + (tall, tall) + (split,) * 4,
        out_specs=outs + outs,
        check_vma=False,
    )
```

profile of v0, /device:TPU:1, one launch (start us, length us, event | category | flops | bytes accessed | tf_op | source)
XLA Modules:
  0.0 151.8 jit_solution(13737360906417343041)
XLA Ops:
  0.6 143.3 %exchange.1 = (f32[16,128]{1,0:T(8,128)}, f32[16,128]{1,0:T(8,128)}, f32[16,128]{1,0:T(8,128)}, f32[16,128]{1,0:T(8,128)}, bf16[2,256,128]{2,1,0:T(8,128)(2,1)},...) custom-call(bf16[1024,128]{1,0:T(8,128)(2,1)} %x_hbm.1, ...), custom_call_target="tpu_custom_call" | custom-call | tf_op jit(solution)/shard_map/exchange/pallas_call | solution.py:402
  144.0 7.9 %final.1 = (f32[256,128]{1,0:T(8,128)}, f32[256,128]{1,0:T(8,128)}, bf16[4096,128]{1,0:T(8,128)(2,1)}, f32[256,128]{1,0:T(8,128)}, f32[256,128]{1,0:T(8,128)}, /...) custom-call(f32[2,8,128]{2,1,0:T(8,128)} %get-tuple-element.28.refs_, ...), custom_call_target="tpu_custom_call" | custom-call | tf_op jit(solution)/shard_map/final/pallas_call | solution.py:460
where the time goes:
time: 152 us
  Pallas kernels  151 us (99%)
    pallas_call x1, Pallas kernels, body(): pl.pallas_call(functools.partial(exchange_kernel, fs, tp), name='exchange...  143 us
    pallas_call x1, Pallas kernels, body(): pl.pallas_call(final_kernel, name='final', out_shape=(big, big, copied) *...  7.86 us

commit v1 on v0

v1 whole, which is shorter than its diff:
```python
import contextlib
import functools

import jax
import jax.numpy as jnp
from jax import lax
from jax.experimental import pallas as pl
from jax.experimental.pallas import tpu as pltpu
from jax.sharding import PartitionSpec as P

HD = 128
SIDE = 4

moment_decay = 0.8
square_decay = 0.9
square_floor = 1.0
norm_floor = 0.01
step_rate = 0.01

BF = jnp.bfloat16
F32 = jnp.float32
MESH = pl.DeviceIdType.MESH
SCOPES = False


def scope(name):
    return jax.named_scope(name) if SCOPES else contextlib.nullcontext()


def wrap(offset):
    return (offset + 1) % SIDE - 1


ARRIVALS = [(-1, 0, None), (1, 0, None), (2, 0, 0), (2, 0, 1)]
for near in (-1, 1):
    ARRIVALS += [(0, near, None), (-1, near, None), (1, near, None), (2, near, 0), (2, near, 1)]
for u in (0, -1, 1, 2):
    ARRIVALS += [(u, 2, 0), (u, 2, 1)]
SLOT = {
    (kind, *key): kind * len(ARRIVALS) + place
    for kind in range(2)
    for place, key in enumerate(ARRIVALS)
}


def forwards(u, v, part):
    onward = []
    if v == 0:
        if u == -1:
            onward.append((0, 0, 1))
        if u == 1:
            onward.append((1, 0, -1))
        onward += [(part, 1, 1), (part, 1, -1)]
    elif v == -1 and part != 1:
        onward.append((0, 1, 1))
    elif v == 1 and part != 0:
        onward.append((1, 1, -1))
    return onward


class Gather:
    def __init__(self, piece, send_sem, recv_sem, x, y, t):
        self.piece, self.send_sem, self.recv_sem = piece, send_sem, recv_sem
        self.x, self.y, self.t = x, y, t
        self.copies = []

    def owner(self, kind, u, v):
        dx, dy = (u, v) if kind == 0 else (v, u)
        return lax.rem(self.y + dy + SIDE, SIDE) * SIDE + lax.rem(self.x + dx + SIDE, SIDE)

    def copy(self, kind, u, v, part, axis, direction):
        step = (direction, 0) if axis == 0 else (0, direction)
        slot = SLOT[kind, wrap(u - step[0]), wrap(v - step[1]), part]
        ref = self.piece(kind, self.owner(kind, u, v), part)
        return pltpu.make_async_remote_copy(
            src_ref=ref,
            dst_ref=ref,
            send_sem=self.send_sem.at[slot],
            recv_sem=self.recv_sem.at[slot],
            device_id=(self.owner(kind, *step), self.t),
            device_id_type=MESH,
        )

    def send(self, kind, u, v, part, axis, direction):
        copy = self.copy(kind, u, v, part, axis, direction)
        copy.start()
        self.copies.append(copy)

    def start(self):
        for axis in range(2):
            for kind in range(2):
                for direction in (1, -1):
                    self.send(kind, 0, 0, None, axis, direction)

    def wait(self, kind, u, v, part):
        ref = self.piece(kind, self.owner(kind, u, v), part)
        slot = SLOT[kind, u, v, part]
        pltpu.make_async_remote_copy(
            src_ref=ref,
            dst_ref=ref,
            send_sem=self.send_sem.at[slot],
            recv_sem=self.recv_sem.at[slot],
            device_id=(self.owner(kind, 1, 0), self.t),
            device_id_type=MESH,
        ).wait_recv()

    def take(self, *keys):
        for u, v, part in keys:
            for kind in range(2):
                self.wait(kind, u, v, part)
                for onward, axis, direction in forwards(u, v, part):
                    self.send(kind, u, v, onward, axis, direction)


STAGES = [
    [(-1, 0, None), (1, 0, None)],
    [(0, -1, None), (0, 1, None)],
    [(2, 0, 0), (2, 0, 1)],
    [(-1, -1, None), (-1, 1, None), (1, -1, None), (1, 1, None)],
    [(2, -1, 0), (2, 1, 1), (2, -1, 1), (2, 1, 0)],
    [(0, 2, 0), (0, 2, 1)],
    [(u, 2, part) for u in (-1, 1, 2) for part in range(2)],
]


def exchange_kernel(
    fs,
    tp,
    x_ref,
    qc_ref,
    kc_ref,
    qm_ref,
    km_ref,
    qb_ref,
    kb_ref,
    qf_ref,
    qs_ref,
    kf_ref,
    ks_ref,
    qfn_ref,
    qsn_ref,
    kfn_ref,
    ksn_ref,
    scale_ref,
    gathered,
    update_ref,
    own_ref,
    ratio_ref,
    basis,
    x_all,
    acc,
    low,
    proj,
    proj_send,
    proj_recv,
    b_send,
    b_recv,
    m_send,
    m_recv,
    x_send,
    x_recv,
    xd_send,
    xd_recv,
    z_send,
    z_recv,
    zd_send,
    zd_recv,
    d_send,
    d_recv,
    rs_send,
    rs_recv,
    ag_send,
    ag_recv,
):
    f = lax.axis_index("fs")
    t = lax.axis_index("tp")
    z, c = t // 2, t % 2
    x, y = f % SIDE, f // SIDE
    partner = (f, t + 1 - 2 * c)
    depth = tp // 2
    rows, rank = qb_ref.shape
    width = qc_ref.shape[1]
    tokens, columns = x_ref.shape
    part_rows = rank // fs
    chunk = tokens // depth
    half = rows // 2

    def at(start, size):
        return pl.ds(pl.multiple_of(start, size), size)

    def remote(src, dst, send, recv, target):
        return pltpu.make_async_remote_copy(
            src_ref=src,
            dst_ref=dst,
            send_sem=send,
            recv_sem=recv,
            device_id=target,
            device_id_type=MESH,
        )

    def along(offset):
        return lax.rem(z + offset + depth, depth)

    sent = []

    def go(copy):
        copy.start()
        sent.append(copy)

    own_rows = at(f * rows, rows)
    with scope("barrier"):
        barrier = pltpu.get_barrier_semaphore()

        def greet(target):
            pl.semaphore_signal(barrier, inc=1, device_id=target, device_id_type=MESH)

        for d in range(1, depth):
            greet((f, along(d) * 2 + c))
        for m in range(1, fs):
            greet((f ^ m, t))
        greet(partner)
        for j, (own_basis, master) in enumerate(((qb_ref, qm_ref), (kb_ref, km_ref))):
            basis[j, own_rows, :] = own_basis[...]
            gathered[j, own_rows, :] = master[...].astype(BF)
        x_all[c, z] = x_ref[at(z * chunk, chunk), :]
        pl.semaphore_wait(barrier, fs - 1 + depth)

    def basis_piece(kind, owner, part):
        start, size = owner * rows + kind * half, half
        if part is not None:
            start, size = start + part * (half // 2), half // 2
        return basis.at[c, at(start, size)]

    def master_piece(kind, owner, part):
        start, size = owner * rows, rows
        if part is not None:
            start, size = start + part * half, half
        return gathered.at[kind, at(start, size)]

    bases = Gather(basis_piece, b_send, b_recv, x, y, t)
    masters = Gather(master_piece, m_send, m_recv, x, y, t)

    bases.start()

    def x_copy(e):
        return remote(
            x_ref.at[at(along(e) * chunk, chunk)],
            x_all.at[c, z],
            x_send.at[e % depth],
            x_recv.at[-e % depth],
            (f, along(e) * 2 + c),
        )

    far = depth // 2
    offsets = [far] + [s * e for e in range(far - 1, 0, -1) for s in (1, -1)]
    for e in offsets:
        go(x_copy(e))
    go(
        remote(
            x_ref.at[at(z * chunk, chunk)], x_all.at[c, z], xd_send.at[0], xd_recv.at[0], partner
        )
    )

    def x_wait(e):
        piece = x_all.at[c, along(e)]
        remote(
            piece, piece, x_send.at[e % depth], x_recv.at[e % depth], (f, along(e) * 2 + c)
        ).wait_recv()

    def x_take(e):
        x_wait(e)
        piece = x_all.at[c, along(e)]
        go(remote(piece, piece, xd_send.at[e % depth], xd_recv.at[e % depth], partner))

    def x_partner(e):
        piece = x_all.at[1 - c, along(e)]
        remote(
            piece, piece, xd_send.at[e % depth], xd_recv.at[e % depth], partner
        ).wait_recv()

    with scope("basis"):
        acc[...] = jnp.zeros_like(acc)
        for stage in STAGES[:5]:
            bases.take(*stage)
    masters.start()
    with scope("x_wait"):
        for e in offsets:
            x_take(e)
    with scope("x_partner"):
        for e in [0] + offsets:
            x_partner(e)

    def project(u, v):
        owner = lax.rem(y + v + SIDE, SIDE) * SIDE + lax.rem(x + u + SIDE, SIDE)
        per = depth * 2 * columns // (fs * rows) * rows // columns
        for i in range(per // 2):
            group = owner * (per // 2) + i
            both = jnp.concatenate([x_all[0, group], x_all[1, group]], axis=1)
            place = at(owner * rows + i * 2 * columns, 2 * columns)
            acc[...] += jnp.dot(both, basis[c, place, :], preferred_element_type=F32)

    with scope("project"):
        for u in (0, -1, 1):
            for v in (0, -1, 1):
                project(u, v)
    with scope("basis_end"):
        for stage in STAGES[5:]:
            bases.take(*stage)
    with scope("project_end"):
        for u in (0, -1, 1, 2):
            project(u, 2)
        for v in (0, -1, 1):
            project(2, v)
        low[c, at(z * chunk, chunk), :] = acc[...].astype(BF)

    def low_rows(e, part=None):
        start, size = along(e) * chunk, chunk
        if part is not None:
            start, size = start + part * (chunk // 2), chunk // 2
        return at(start, size)

    def z_slot(e, part=None):
        return depth if part == 1 else e % depth

    def z_go(e, hop, part=None):
        piece = low.at[c, low_rows(e, part)]
        slot = z_slot(e - hop, part)
        go(
            remote(
                piece, piece, z_send.at[slot], z_recv.at[slot], (f, along(hop) * 2 + c)
            )
        )

    def z_wait(e, part=None):
        piece = low.at[c, low_rows(e, part)]
        slot = z_slot(e, part)
        remote(piece, piece, z_send.at[slot], z_recv.at[slot], partner).wait_recv()

    def z_partner(e, j):
        piece = low.at[j, low_rows(e)]
        return remote(piece, piece, zd_send.at[e % depth], zd_recv.at[e % depth], partner)

    def spread(e, sign):
        reach = abs(e)
        if reach + 2 < far:
            z_go(e, 2 * sign)
        elif reach + 2 == far:
            z_go(e, 2 * sign, 0 if sign > 0 else 1)
        z_go(e, sign)

    def z_take(e):
        z_wait(e)
        if abs(e) % 2 == 0 and abs(e) < far:
            spread(e, 1 if e < 0 else -1)
        go(z_partner(e, c))

    def share(m):
        piece = basis.at[c, at((f ^ m) * rows, rows)]
        return remote(piece, piece, d_send.at[m], d_recv.at[m], partner)

    with scope("z_start"):
        for sign in (1, -1):
            spread(0, sign)
        go(z_partner(0, c))
        for m in range(1, fs):
            go(share(m))

    with scope("z_gather"):
        masters.take(*STAGES[0])
        masters.take(*STAGES[1])
        reach = 2
        stage = 2
        while reach < far:
            for e in (-reach, reach, 1 - reach, reach - 1):
                z_take(e)
            if stage < 5:
                masters.take(*STAGES[stage])
                stage += 1
            reach += 2
        for e in (1 - far, far - 1):
            z_take(e)
        z_wait(far, 0)
        z_wait(far, 1)
        go(z_partner(far, c))
    with scope("z_partner"):
        for e in [0] + offsets:
            z_partner(e, 1 - c).wait_recv()

    with scope("low"):
        for j, cot in enumerate((qc_ref, kc_ref)):
            product = lax.dot_general(
                low[j], cot[...], (((0,), (0,)), ((), ())), preferred_element_type=F32
            )
            proj[j] = product
            proj_send[j] = product.astype(BF)
    with scope("reduce"):
        for m in range(fs - 1, 0, -1):
            go(
                remote(
                    proj_send.at[:, at((f ^ m) * part_rows, part_rows)],
                    proj_recv.at[m],
                    rs_send.at[m],
                    rs_recv.at[m],
                    (f ^ m, t),
                )
            )
        while stage < len(STAGES):
            masters.take(*STAGES[stage])
            stage += 1
        for m in range(1, fs):
            remote(
                proj_recv.at[m], proj_recv.at[m], rs_send.at[m], rs_recv.at[m], (f ^ m, t)
            ).wait_recv()

    own = at(f * part_rows, part_rows)
    with scope("moments"):
        moments = ((qf_ref, qs_ref, qfn_ref, qsn_ref), (kf_ref, ks_ref, kfn_ref, ksn_ref))
        for j, (first, second, first_out, second_out) in enumerate(moments):
            summed = proj[j, own, :]
            for m in range(1, fs):
                summed = summed + proj_recv[m, j].astype(F32)
            first_new = moment_decay * first[...] + (1.0 - moment_decay) * summed
            second_new = square_decay * second[...] + (1.0 - square_decay) * summed * summed
            first_out[...] = first_new
            second_out[...] = second_new
            ratio_ref[j, own, :] = (first_new / jnp.sqrt(second_new + square_floor)).astype(BF)

    def ratio_copy(m, owner):
        piece = ratio_ref.at[:, at(owner * part_rows, part_rows)]
        return remote(piece, piece, ag_send.at[m], ag_recv.at[m], (f ^ m, t))

    with scope("ratio"):
        for m in range(fs - 1, 0, -1):
            go(ratio_copy(m, f))
        for m in range(1, fs):
            piece = basis.at[1 - c, at((f ^ m) * rows, rows)]
            remote(piece, piece, d_send.at[m], d_recv.at[m], partner).wait_recv()
        for m in range(1, fs):
            ratio_copy(m, f ^ m).wait_recv()

    with scope("update"):
        high = min(fs * rows, 512)
        for j in range(2):

            def add(i, total, j=j):
                place = at(i * high, high)
                update = jnp.dot(
                    basis[j, place, :], ratio_ref[j], preferred_element_type=F32
                )
                update_ref[j, place, :] = update
                return total + jnp.sum((update * update).reshape(high // 8, 8, width), axis=0)

            sums = lax.fori_loop(0, fs * rows // high, add, jnp.zeros((8, width), F32))
            sums = jnp.sum(sums, axis=0, keepdims=True)
            for h in range(width // HD):
                head = slice(h * HD, (h + 1) * HD)
                total = jnp.sum(sums[:, head], axis=1, keepdims=True)
                scale = 1.0 / jnp.sqrt(total / (fs * rows * HD) + norm_floor)
                scale_ref[j, :, head] = jnp.broadcast_to(scale, (8, HD))
            own_ref[j] = update_ref[j, own_rows, :]

    with scope("drain"):
        for copy in sent + bases.copies + masters.copies:
            copy.wait_send()


def final_kernel(scale_ref, update_ref, gathered_ref, own_ref, qm_ref, km_ref, *refs):
    moments, outs, moments_out = refs[:4], refs[4:10], refs[10:]
    for j, master in enumerate((qm_ref, km_ref)):
        scale = scale_ref[j, 0:1, :]
        step_out, weight_out, copy_out = outs[3 * j : 3 * j + 3]
        step = own_ref[j] * scale
        step_out[...] = step
        weight_out[...] = master[...] - step_rate * step
        step = update_ref[j] * scale
        copy_out[...] = (gathered_ref[j].astype(F32) - step_rate * step).astype(BF)

    @pl.when(pl.program_id(0) == 0)
    def _():
        for source, target in zip(moments, moments_out):
            target[...] = source[...]


def body(fs, tp, *args):
    saved_input, query_cot, _, query_master, key_master, query_basis, key_basis = args[:7]
    rows, rank = query_basis.shape
    tokens, columns = saved_input.shape
    width = query_cot.shape[1]
    part = rank // fs
    depth = tp // 2
    count = fs * rows
    chunk = tokens // depth
    vmem = pl.BlockSpec(memory_space=pltpu.VMEM)
    dma = pltpu.SemaphoreType.DMA
    moment = jax.ShapeDtypeStruct((part, width), F32)
    pairs = []
    slots = (2 * len(ARRIVALS), 2 * len(ARRIVALS), depth, depth, depth + 1, depth, fs, fs, fs)
    for slot in slots:
        pairs += [dma((slot,)), dma((slot,))]
    results = pl.pallas_call(
        functools.partial(exchange_kernel, fs, tp),
        name="exchange",
        out_shape=(
            moment,
            moment,
            moment,
            moment,
            jax.ShapeDtypeStruct((2, 8, width), F32),
            jax.ShapeDtypeStruct((2, count, width), BF),
            jax.ShapeDtypeStruct((2, count, width), F32),
            jax.ShapeDtypeStruct((2, rows, width), F32),
        ),
        in_specs=[vmem] * 11,
        out_specs=(vmem,) * 8,
        scratch_shapes=[
            pltpu.VMEM((2, rank, width), BF),
            pltpu.VMEM((2, count, rank), BF),
            pltpu.VMEM((2, depth, chunk, columns), BF),
            pltpu.VMEM((chunk, rank), F32),
            pltpu.VMEM((2, tokens, rank), BF),
            pltpu.VMEM((2, rank, width), F32),
            pltpu.VMEM((2, rank, width), BF),
            pltpu.VMEM((fs, 2, part, width), BF),
            *pairs,
        ],
        compiler_params=pltpu.CompilerParams(
            collective_id=0, has_side_effects=True, vmem_limit_bytes=24 * 1024 * 1024
        ),
    )(*args)
    moments, (scale, gathered, update, own) = results[:4], results[4:]

    steps = min(8, rows // 16)
    own_tile, tile = rows // steps, count // steps

    def row(i):
        return (i, 0)

    def pair(i):
        return (0, i, 0)

    def whole(i):
        return (0, 0, 0)

    own_spec = pl.BlockSpec((own_tile, width), row)
    full_spec = pl.BlockSpec((tile, width), row)
    moment_spec = pl.BlockSpec((part, width), lambda i: (0, 0))
    big = jax.ShapeDtypeStruct((rows, width), F32)
    copied = jax.ShapeDtypeStruct((count, width), BF)
    outs = pl.pallas_call(
        final_kernel,
        name="final",
        out_shape=(big, big, copied) * 2 + (moment,) * 4,
        grid=(steps,),
        in_specs=[
            pl.BlockSpec((2, 8, width), whole),
            pl.BlockSpec((2, tile, width), pair),
            pl.BlockSpec((2, tile, width), pair),
            pl.BlockSpec((2, own_tile, width), pair),
            own_spec,
            own_spec,
        ]
        + [moment_spec] * 4,
        out_specs=(own_spec, own_spec, full_spec) * 2 + (moment_spec,) * 4,
        compiler_params=pltpu.CompilerParams(vmem_limit_bytes=24 * 1024 * 1024),
    )(scale, update, gathered, own, query_master, key_master, *moments)
    return (*outs[:3], *outs[6:8], *outs[3:6], *outs[8:])


def solution(mesh):
    split, tall, wide = P("fs", "tp"), P("fs", None), P(None, "tp")
    outs = (split, split, wide, split, split)
    return jax.shard_map(
        functools.partial(body, mesh.shape["fs"], mesh.shape["tp"]),
        mesh=mesh,
        in_specs=(split,) * 5 + (tall, tall) + (split,) * 4,
        out_specs=outs + outs,
        check_vma=False,
    )
```

time: 152 us -> 83.3 us (0.55)
  Pallas kernels: 151 us -> 72.9 us
  local copies, waits for them, and re-layouts: 0 us -> 9.24 us
    pallas_call x1, Pallas kernels: 143 us -> 69.1 us  [body(): pl.pallas_call(functools.partial(exchange_kernel, fs, tp), name='exchange...]
    unnamed x0 -> x22, local copies, waits for them, and re-layouts: none -> 9.24 us
    pallas_call x1, Pallas kernels: 7.86 us -> 3.78 us  [body(): pl.pallas_call(final_kernel, name='final', out_shape=(big, big, copied) *...]
where the time goes in v1:
time: 83.3 us; the launch traced here: 82.8 us
  Pallas kernels  72.9 us (88%)
  local copies, waits for them, and re-layouts  9.24 us (11%)
    pallas_call x1, Pallas kernels, body(): pl.pallas_call(functools.partial(exchange_kernel, fs, tp), name='exchange...  69.1 us
    unnamed x22, local copies, waits for them, and re-layouts  9.24 us
    pallas_call x1, Pallas kernels, body(): pl.pallas_call(final_kernel, name='final', out_shape=(big, big, copied) *...  3.78 us

profile of v1, /device:TPU:1, one launch (start us, length us, event | category | flops | bytes accessed | tf_op | source)
XLA Modules:
  0.0 82.8 jit_solution(15612000981633803350)
XLA Ops:
  0.6 0.0 copy-start
  0.7 0.9 %copy-done = f32[256,128]{1,0:T(8,128)S(1)} copy-done((f32[256,128]{1,0:T(8,128)S(1)}, f32[256,128]{1,0:T(8,128)}, u32[]{:S(2)}) %copy-start) | copy-done | bytes 131096
  1.6 0.0 copy-start.1
  1.6 0.9 %copy-done.1 = f32[256,128]{1,0:T(8,128)S(1)} copy-done((f32[256,128]{1,0:T(8,128)S(1)}, f32[256,128]{1,0:T(8,128)}, u32[]{:S(2)}) %copy-start.1) | copy-done | bytes 131096
  2.5 0.0 copy-start.2
  2.5 0.9 %copy-done.2 = bf16[1024,128]{1,0:T(8,128)(2,1)S(1)} copy-done((bf16[1024,128]{1,0:T(8,128)(2,1)S(1)}, bf16[1024,128]{1,0:T(8,128)(2,1)}, u32[]{:S(2)}) %copy-start.2) | copy-done | bytes 262168
  3.4 0.0 copy-start.3
  3.4 0.9 %copy-done.3 = bf16[1024,128]{1,0:T(8,128)(2,1)S(1)} copy-done((bf16[1024,128]{1,0:T(8,128)(2,1)S(1)}, bf16[1024,128]{1,0:T(8,128)(2,1)}, u32[]{:S(2)}) %copy-start.3) | copy-done | bytes 262168
  4.4 0.0 copy-start.4
  4.4 0.9 %copy-done.4 = bf16[1024,128]{1,0:T(8,128)(2,1)S(1)} copy-done((bf16[1024,128]{1,0:T(8,128)(2,1)S(1)}, bf16[1024,128]{1,0:T(8,128)(2,1)}, u32[]{:S(2)}) %copy-start.4) | copy-done | bytes 262168
  5.3 0.0 copy-start.5
  5.3 0.9 %copy-done.5 = bf16[256,256]{1,0:T(8,128)(2,1)S(1)} copy-done((bf16[256,256]{1,0:T(8,128)(2,1)S(1)}, bf16[256,256]{1,0:T(8,128)(2,1)}, u32[]{:S(2)}) %copy-start.5) | copy-done | bytes 131096
  6.2 0.0 copy-start.6
  6.2 0.9 %copy-done.6 = bf16[256,256]{1,0:T(8,128)(2,1)S(1)} copy-done((bf16[256,256]{1,0:T(8,128)(2,1)S(1)}, bf16[256,256]{1,0:T(8,128)(2,1)}, u32[]{:S(2)}) %copy-start.6) | copy-done | bytes 131096
  7.1 0.0 copy-start.7
  7.1 0.7 copy-done.7
  7.8 0.0 copy-start.8
  7.8 0.7 copy-done.8
  8.5 0.0 copy-start.9
  8.5 0.7 copy-done.9
  9.2 0.0 copy-start.10
  9.2 0.7 copy-done.10
  9.9 69.1 %exchange.1 = (f32[16,128]{1,0:T(8,128)S(1)}, f32[16,128]{1,0:T(8,128)S(1)}, f32[16,128]{1,0:T(8,128)S(1)}, f32[16,128]{1,0:T(8,128)S(1)}, f32[2,8,128]{2,1,0:T(...) custom-call(bf16[1024,128]{1,0:T(8,128)(2,1)S(1)} %copy-done.2, ...), custom_call_target="tpu_custom_call" | custom-call | tf_op jit(solution)/shard_map/exchange/pallas_call | solution.py:500
  79.0 3.8 %final.1 = (f32[256,128]{1,0:T(8,128)}, f32[256,128]{1,0:T(8,128)}, bf16[4096,128]{1,0:T(8,128)(2,1)}, f32[256,128]{1,0:T(8,128)}, f32[256,128]{1,0:T(8,128)}, /...) custom-call(f32[2,8,128]{2,1,0:T(8,128)S(1)} %get-tuple-element.28.s, ...), custom_call_target="tpu_custom_call" | custom-call | tf_op jit(solution)/shard_map/final/pallas_call | solution.py:549
Async XLA Ops:
  0.6 0.9 %copy-start = (f32[256,128]{1,0:T(8,128)S(1)}, f32[256,128]{1,0:T(8,128)}, u32[]{:S(2)}) copy-start(f32[256,128]{1,0:T(8,128)} %qm_ref.3) | copy-start | bytes 393220
  1.6 0.9 %copy-start.1 = (f32[256,128]{1,0:T(8,128)S(1)}, f32[256,128]{1,0:T(8,128)}, u32[]{:S(2)}) copy-start(f32[256,128]{1,0:T(8,128)} %km_ref.3) | copy-start | bytes 393220
  2.5 0.9 %copy-start.2 = (bf16[1024,128]{1,0:T(8,128)(2,1)S(1)}, bf16[1024,128]{1,0:T(8,128)(2,1)}, u32[]{:S(2)}) copy-start(bf16[1024,128]{1,0:T(8,128)(2,1)} %x_ref.1) | copy-start | bytes 786436
  3.4 0.9 %copy-start.3 = (bf16[1024,128]{1,0:T(8,128)(2,1)S(1)}, bf16[1024,128]{1,0:T(8,128)(2,1)}, u32[]{:S(2)}) copy-start(bf16[1024,128]{1,0:T(8,128)(2,1)} %qc_ref.1) | copy-start | bytes 786436
  4.4 0.9 %copy-start.4 = (bf16[1024,128]{1,0:T(8,128)(2,1)S(1)}, bf16[1024,128]{1,0:T(8,128)(2,1)}, u32[]{:S(2)}) copy-start(bf16[1024,128]{1,0:T(8,128)(2,1)} %kc_ref.1) | copy-start | bytes 786436
  5.3 0.9 %copy-start.5 = (bf16[256,256]{1,0:T(8,128)(2,1)S(1)}, bf16[256,256]{1,0:T(8,128)(2,1)}, u32[]{:S(2)}) copy-start(bf16[256,256]{1,0:T(8,128)(2,1)} %qb_ref.1) | copy-start | bytes 393220
  6.2 0.9 %copy-start.6 = (bf16[256,256]{1,0:T(8,128)(2,1)S(1)}, bf16[256,256]{1,0:T(8,128)(2,1)}, u32[]{:S(2)}) copy-start(bf16[256,256]{1,0:T(8,128)(2,1)} %kb_ref.1) | copy-start | bytes 393220
  7.1 0.7 copy-start.7
  7.8 0.7 copy-start.8
  8.5 0.7 copy-start.9
  9.2 0.7 copy-start.10
